TPU v7x, 32 devices: a whole 2x2x4 slice. The times are simulated.
32 devices in a mesh: sp: 4 (over z), dp: 8 (over y, x, core).
Axes of the slice: x: 2, y: 2, z: 4, core: 2. Of those that a mesh axis runs over, the one named last changes fastest.
Arguments:
- query_rows: bfloat16 [8, 512, 1024], P('dp', 'sp'), may hold values from -5.5 to 5.5
- key_rows: bfloat16 [8, 512, 1024], P('dp', 'sp'), may hold values from -5.5 to 5.5
- value_rows: bfloat16 [8, 512, 1024], P('dp', 'sp'), may hold values from -6 to 6
- lambdas: float32 [8], replicated, may hold values from 0.3 to 0.8
- query_gain: float32 [64], replicated, may hold values from 1.1 to 8
- key_gain: float32 [64], replicated, may hold values from 1.1 to 8
- sub_gain: float32 [128], replicated, may hold values from 0.1 to 1.9
- out_weight: bfloat16 [1024, 2048], P(None, 'dp'), may hold values from -0.1875 to 0.1875
Outputs:
- attended: bfloat16 [8, 512, 2048], P('dp', 'sp')
All inputs are finite; a program needn't handle non-finite values.
Results may differ from a plain program's by a relative error of at most 0.0025.
The roundings to bfloat16 on the way count: a program that leaves them out, or rounds other values in their place, can miss the bound.
Values may be sent and summed in bfloat16 or wider, within the bound.
A program may use at most 64 MiB of HBM per device.

v0:
```python
import functools

import jax
import jax.numpy as jnp
from jax import lax
from jax.experimental import pallas as pl
from jax.experimental.pallas import tpu as pltpu
from jax.sharding import PartitionSpec as P

D = 2048
HEADS = 8
HK = 64
HV = 128


epsilon = 1e-06
output_scale = 0.8


def normalize(field, scaling):
    return field * lax.rsqrt(jnp.mean(field * field, axis=-1, keepdims=True) + epsilon) * scaling


def attend(arrived, length):
    block_rows = max(min(512, length), length // 16)
    results = []
    for number in range(length // block_rows):
        first_row = number * block_rows
        last_row = first_row + block_rows
        query_block = arrived[first_row:last_row, :, :HK]
        key_block = arrived[:last_row, :, HK : 2 * HK]
        value_block = arrived[:last_row, :, 2 * HK :]
        scores = jnp.einsum(
            "qgd,kgd->gqk", query_block, key_block, preferred_element_type=jnp.float32
        ) * HK ** (-0.5)
        visible = jnp.arange(last_row)[None, :] <= (first_row + jnp.arange(block_rows))[:, None]
        scores = jnp.where(visible[None], scores, -jnp.inf)
        weights = jax.nn.softmax(scores, axis=-1).astype(jnp.bfloat16)
        results.append(
            jnp.einsum(
                "gqk,kgd->qgd", weights, value_block, preferred_element_type=jnp.float32
            ).astype(jnp.bfloat16)
        )
    return jnp.concatenate(results, axis=0)


def body(query_rows, key_rows, value_rows, lambdas, query_gain, key_gain, sub_gain, out_weight):
    sequences = query_rows.shape[0]
    tokens_here = query_rows.shape[1]
    groups = 2 * HEADS
    query_norm = normalize(
        query_rows.reshape(sequences, tokens_here, groups, HK).astype(jnp.float32), query_gain
    ).astype(jnp.bfloat16)
    key_norm = normalize(
        key_rows.reshape(sequences, tokens_here, groups, HK).astype(jnp.float32), key_gain
    ).astype(jnp.bfloat16)
    value_heads = value_rows.reshape(sequences, tokens_here, HEADS, HV)
    packet = jnp.concatenate(
        [query_norm, key_norm, jnp.concatenate([value_heads, value_heads], axis=2)], axis=3
    )
    arrived = lax.all_to_all(packet, "sp", split_axis=2, concat_axis=1, tiled=True)
    length = arrived.shape[1]
    map_outputs = attend(arrived[0], length)[None]
    returned = lax.all_to_all(map_outputs, "sp", split_axis=1, concat_axis=2, tiled=True)
    returned_float = returned.astype(jnp.float32)
    mixed_heads = returned_float[:, :, :HEADS] - lambdas[:, None] * returned_float[:, :, HEADS:]
    normed = (
        (normalize(mixed_heads, sub_gain) * output_scale)
        .astype(jnp.bfloat16)
        .reshape(sequences * tokens_here, HEADS * HV)
    )
    projected = jnp.dot(
        normed,
        lax.all_gather(out_weight, "dp", axis=1, tiled=True),
        preferred_element_type=jnp.float32,
    )
    return projected.astype(jnp.bfloat16).reshape(sequences, tokens_here, D)


MESH = pl.DeviceIdType.MESH


def fits(sp, dp, rows_shape, weight_shape):
    if sp != 4 or HEADS % sp or (HEADS // sp * HK) % 128 or dp % 2:
        return False
    return rows_shape[0] == 1 and rows_shape[1] % 128 == 0 and rows_shape[1] * sp <= 1024 and weight_shape[1] % 128 == 0


def kernel(
    sp, dp, q_ref, k_ref, v_ref, lam_in, qg_in, kg_in, sg_in, w_ref, out_ref,
    qb, kb, vb, kn, qx, kx, vx, knx, nsend, nbuf, wbuf,
    local_sem, in_send, in_recv, back_send, back_recv, w_send, w_recv, p_send, p_recv, own_sem,
    lam_ref, qg_ref, kg_ref, sg_ref, small_sem, acc,
):
    me, d = lax.axis_index("sp"), lax.axis_index("dp")
    partner = d + 1 - 2 * lax.rem(d, 2)
    chips = dp // 2
    rows = q_ref.shape[0]
    local = HEADS // sp
    width, vwidth = local * HK, local * HV
    depth, columns = w_ref.shape
    half = depth // 2
    square = chips == 4

    def fellow(c, device=d):
        if not square:
            return lax.rem(device + 2 * c, dp)
        core, chip = lax.rem(device, 2), device // 2
        x, y = lax.rem(chip, 2), chip // 2
        x = 1 - x if c % 2 else x
        y = 1 - y if c // 2 else y
        return (y * 2 + x) * 2 + core

    barrier = pltpu.get_barrier_semaphore()
    for o in range(1, sp):
        pl.semaphore_signal(barrier, inc=1, device_id=(lax.rem(me + o, sp), d), device_id_type=MESH)
    for c in range(1, chips):
        pl.semaphore_signal(barrier, inc=1, device_id=(me, fellow(c)), device_id_type=MESH)
    pl.semaphore_signal(barrier, inc=1, device_id=(me, partner), device_id_type=MESH)

    half_sp = sp // 2
    lows, highs = range(half_sp), range(half_sp, sp)

    def at(i):
        return pl.ds(i * rows, rows)

    def cols(pair_, m=0, count=1):
        return pl.ds(m * HEADS * HK + pair_ * width, count * width)

    def vcols(pair_, count=1):
        return pl.ds(pair_ * vwidth, count * vwidth)

    plan = {}
    for z in range(sp):
        for o in range(sp):
            for m in range(2):
                if o != z and (o in lows or z in highs):
                    plan[z, o, "q", m] = q_ref.at[:, cols(o, m)], qb.at[m, at(z), :]
                if o != z and (o in lows or z != 0):
                    plan[z, o, "k", m] = k_ref.at[:, cols(o, m)], kb.at[m, at(z), :]
            if o != z and (o in lows or z != 0):
                plan[z, o, "v", 0] = v_ref.at[:, vcols(o)], vb.at[at(z), :]
    for m in range(2):
        plan[0, 1, "kx", m] = k_ref.at[:, cols(half_sp, m, half_sp)], kx.at[m, at(0), :]
    plan[0, 1, "vx", 0] = v_ref.at[:, vcols(half_sp, half_sp)], vx.at[at(0), :]
    for o in highs:
        for m in range(2):
            plan[1, o, "rk", m] = kx.at[m, at(0), cols(o - half_sp)], kb.at[m, at(0), :]
        plan[1, o, "rv", 0] = vx.at[at(0), vcols(o - half_sp)], vb.at[at(0), :]
    number = {key: n for n, key in enumerate(plan)}

    def move(*key):
        src, dst = plan[key]
        n = number[key]
        return pltpu.make_async_remote_copy(
            src_ref=src, dst_ref=dst, send_sem=in_send.at[n], recv_sem=in_recv.at[n],
            device_id=(key[1], d), device_id_type=MESH,
        )

    def rows_in(z):
        copies = []
        for m in range(2):
            copies.append((k_ref.at[:, cols(z, m)], kb.at[m, at(z), :]))
            copies.append((q_ref.at[:, cols(z, m)], qb.at[m, at(z), :]))
            if z in lows:
                copies.append((k_ref.at[:, cols(half_sp, m, half_sp)], kx.at[m, at(z), :]))
                copies.append((q_ref.at[:, cols(half_sp, m, half_sp)], qx.at[m]))
        copies.append((v_ref.at[:, vcols(z)], vb.at[at(z), :]))
        if z in lows:
            copies.append((v_ref.at[:, vcols(half_sp, half_sp)], vx.at[at(z), :]))
        return [pltpu.make_async_copy(src, dst, local_sem.at[n]) for n, (src, dst) in enumerate(copies)]

    five = (("k", 0), ("q", 0), ("v", 0), ("k", 1), ("q", 1))
    three = (("k", 0), ("v", 0), ("k", 1))

    def outgoing(z):
        if z == 0:
            return [(0, 1, "kx", 0), (0, 1, "vx", 0), (0, 1, "kx", 1)] + [(0, 1) + f for f in five]
        if z == 1:
            return [(1, o) + f for f in three for o in highs] + [(1, 0) + f for f in five]
        if z == 2:
            return [(2, 0) + f for f in five] + [(2, 1) + f for f in five] + [(2, 3) + f for f in five]
        return [(3, 0) + f for f in five] + [(3, 1) + f for f in five] + [(3, 2) + f for f in five]

    relays = (("kx", "rk", 0), ("vx", "rv", 0), ("kx", "rk", 1))

    def rows_of(h):
        return pl.ds(h * half, half)

    def spread(c, h):
        source, over = d, c
        if square and c == 3:
            source, over = fellow(1 + h), 2 - h
        src = w_ref if source is d else wbuf.at[source]
        return pltpu.make_async_remote_copy(
            src_ref=src.at[rows_of(h)], dst_ref=wbuf.at[source, rows_of(h)], send_sem=w_send.at[c, h], recv_sem=w_recv.at[c, h],
            device_id=(me, fellow(over)), device_id_type=MESH,
        )

    def shard_of(device, c):
        if c == 0:
            return device
        return fellow(c, device) if square else lax.rem(device - 2 * c + dp, dp)

    def own_weights():
        return pltpu.make_async_copy(w_ref, wbuf.at[d], own_sem)

    def gained(c, h):
        at = shard_of(d, c)
        pltpu.make_async_remote_copy(
            src_ref=wbuf.at[at, rows_of(h)], dst_ref=wbuf.at[at, rows_of(h)], send_sem=w_send.at[c, h], recv_sem=w_recv.at[c, h],
            device_id=(me, partner), device_id_type=MESH,
        ).wait_recv()

    def pair(c):
        at = shard_of(d, c)
        return pltpu.make_async_remote_copy(
            src_ref=w_ref if c == 0 else wbuf.at[at], dst_ref=wbuf.at[at],
            send_sem=p_send.at[c], recv_sem=p_recv.at[c],
            device_id=(me, partner), device_id_type=MESH,
        )

    def back(z, i):
        return pltpu.make_async_remote_copy(
            src_ref=nsend.at[i], dst_ref=nbuf.at[z], send_sem=back_send.at[i], recv_sem=back_recv.at[z],
            device_id=(i, d), device_id_type=MESH,
        )

    small = [
        pltpu.make_async_copy(src, dst, small_sem.at[n])
        for n, (src, dst) in enumerate(((lam_in, lam_ref), (qg_in, qg_ref), (kg_in, kg_ref), (sg_in, sg_ref)))
    ]
    for z in range(sp):
        @pl.when(me == z)
        def _(z=z):
            for copy in rows_in(z):
                copy.start()
    own_weights().start()
    for copy in small:
        copy.start()
    pl.semaphore_wait(barrier, sp - 1 + chips)

    for z in range(sp):
        @pl.when(me == z)
        def _(z=z):
            for key in outgoing(z):
                move(*key).start()

    for order in range(2):
        for c in range(1, chips):
            if not (square and c == 3):
                spread(c, (c + 1 + order) % 2).start()
    pair(0).start()
    for copy in small:
        copy.wait()

    def weights_first():
        if square:
            for h in range(2):
                gained(1 + h, h)
                spread(3, h).start()

    def weights_next():
        if square:
            for h in range(2):
                gained(1 + h, 1 - h)
                pair(1 + h).start()

    def weights_last():
        for c in range(3 if square else 1, chips):
            for h in range(2):
                gained(c, h)
            pair(c).start()

    lane = lax.broadcasted_iota(jnp.int32, (width, width), 1) // HK
    ones = (lane == lax.broadcasted_iota(jnp.int32, (width, width), 0) // HK).astype(jnp.bfloat16)
    head_of = lax.broadcasted_iota(jnp.int32, (rows, width), 1) // HK
    visible = lax.broadcasted_iota(jnp.int32, (rows, rows), 1) <= lax.broadcasted_iota(jnp.int32, (rows, rows), 0)
    visible = jnp.concatenate([visible] * local, axis=0)
    query_gain = jnp.concatenate([qg_ref[...]] * local, axis=1)
    key_gain = jnp.concatenate([kg_ref[...]] * local, axis=1)
    sub_gain = sg_ref[...] * output_scale

    def normed_rows(block, gain):
        field = block.astype(jnp.float32)
        square = field * field
        upper = square.astype(jnp.bfloat16)
        lower = (square - upper.astype(jnp.float32)).astype(jnp.bfloat16)
        total = jnp.dot(upper, ones, preferred_element_type=jnp.float32)
        total += jnp.dot(lower, ones, preferred_element_type=jnp.float32)
        return (field * lax.rsqrt(total * (1.0 / HK) + epsilon) * gain).astype(jnp.bfloat16)

    def attend(query, keys, vals, before):
        query = normed_rows(query, query_gain)
        zero = jnp.zeros_like(query)
        stacked = jnp.concatenate([jnp.where(head_of == h, query, zero) for h in range(local)], axis=0)
        scores = lax.dot_general(
            stacked, keys, (((1,), (1,)), ((), ())), preferred_element_type=jnp.float32
        ) * HK ** (-0.5)
        last = jnp.where(visible, scores[:, before:], -jnp.inf)
        scores = last if before == 0 else jnp.concatenate([scores[:, :before], last], axis=1)
        raised = jnp.exp(scores - jnp.max(scores, axis=1, keepdims=True))
        weights = (raised * (1.0 / jnp.sum(raised, axis=1, keepdims=True))).astype(jnp.bfloat16)
        return [
            jnp.dot(
                weights[h * rows : (h + 1) * rows], vals[:, h * HV : (h + 1) * HV],
                preferred_element_type=jnp.float32,
            ).astype(jnp.bfloat16)
            for h in range(local)
        ]

    def mix(pair_, maps):
        parts = []
        for h in range(local):
            mixed = maps[0][h].astype(jnp.float32) - lam_ref[pair_ * local + h] * maps[1][h].astype(jnp.float32)
            mean = jnp.mean(mixed * mixed, axis=1, keepdims=True)
            parts.append((mixed * lax.rsqrt(mean + epsilon) * sub_gain).astype(jnp.bfloat16))
        return jnp.concatenate(parts, axis=1)

    def new_keys(m, i):
        kn[m, i * rows : (i + 1) * rows, :] = normed_rows(kb[m, i * rows : (i + 1) * rows, :], key_gain)

    def pair_map(m, i):
        keys = (i + 1) * rows
        return attend(qb[m, i * rows : keys, :], kn[m, :keys, :], vb[:keys, :], i * rows)

    def near(z):
        keys = (z + 1) * rows
        for p in range(half_sp):
            maps = []
            for m in range(2):
                for i in range(z + 1):
                    knx[m, i * rows : (i + 1) * rows, :] = normed_rows(
                        kx[m, i * rows : (i + 1) * rows, p * width : (p + 1) * width], key_gain
                    )
                maps.append(attend(
                    qx[m, :, p * width : (p + 1) * width], knx[m, :keys, :],
                    vx[:keys, p * vwidth : (p + 1) * vwidth], z * rows,
                ))
            nbuf[half_sp + p] = mix(half_sp + p, maps)

    def give(z, i, maps):
        if i == z:
            nbuf[z] = mix(z, maps)
        else:
            nsend[i] = mix(z, maps)
            back(z, i).start()

    def below(z):
        for copy in rows_in(z):
            copy.wait()
        if z == 1:
            for held, sent, m in relays:
                move(0, 1, held, m).wait_recv()
                for o in highs:
                    move(1, o, sent, m).start()
        weights_first()
        near(z)
        for i in range(sp):
            maps = []
            for m in range(2):
                if i != z:
                    for f in five[3 * m : 3 + 2 * m]:
                        move(i, z, *f).wait_recv()
                new_keys(m, i)
                maps.append(pair_map(m, i))
            give(z, i, maps)
            if i == half_sp:
                weights_next()

    def above(z):
        for copy in rows_in(z):
            copy.wait()
        weights_first()
        weights_next()
        other = half_sp + sp - 1 - z
        both = {i: [] for i in highs}
        for m in range(2):
            for f in five[3 * m : 3 + 2 * m]:
                move(other, z, *f).wait_recv()
                if f[0] != "q":
                    move(1, z, *f).wait_recv()
                    move(0 + 1, z, "r" + f[0], f[1]).wait_recv()
            for i in range(sp):
                new_keys(m, i)
            for i in (other, z):
                both[i].append(pair_map(m, i))
        for i in (other, z):
            give(z, i, both[i])

    for z in range(sp):
        @pl.when(me == z)
        def _(z=z):
            below(z) if z in lows else above(z)

    def gather_back(owners):
        for z in range(sp):
            @pl.when(me == z)
            def _(z=z):
                for o in owners:
                    if o != z and (o in lows or z in highs):
                        back(o, z).wait_recv()

    def project(shard, owners, first):
        normed = jnp.concatenate([nbuf[j] for j in owners], axis=1)
        weight = wbuf[shard, owners[0] * vwidth : (owners[-1] + 1) * vwidth, :]
        here = pl.ds(pl.multiple_of(shard * columns, 128), columns)
        total = jnp.dot(normed, weight, preferred_element_type=jnp.float32)
        if first:
            acc[:, here] = total
        else:
            out_ref[:, here] = (acc[:, here] + total).astype(jnp.bfloat16)

    weights_last()
    gather_back(highs)
    own_weights().wait()
    for c in range(chips):
        project(shard_of(d, c), highs, True)
    for c in range(chips):
        at_ = shard_of(partner, c)
        pltpu.make_async_remote_copy(
            src_ref=wbuf.at[at_], dst_ref=wbuf.at[at_], send_sem=p_send.at[c], recv_sem=p_recv.at[c],
            device_id=(me, partner), device_id_type=MESH,
        ).wait_recv()
        project(at_, highs, True)
    gather_back(lows)
    for c in range(chips):
        project(shard_of(d, c), lows, False)
        project(shard_of(partner, c), lows, False)

    for z in range(sp):
        @pl.when(me == z)
        def _(z=z):
            for key in outgoing(z):
                move(*key).wait_send()
            if z == 1:
                for _, sent, m in relays:
                    for o in highs:
                        move(1, o, sent, m).wait_send()
            for i in range(sp):
                if i != z and (z in lows or i in highs):
                    back(z, i).wait_send()
    for c in range(chips):
        pair(c).wait_send()
        if c:
            for h in range(2):
                spread(c, h).wait_send()


def fused(sp, dp, query_rows, key_rows, value_rows, lambdas, query_gain, key_gain, sub_gain, out_weight):
    rows = query_rows.shape[1]
    length = rows * sp
    local = HEADS // sp
    width, vwidth = local * HK, local * HV
    depth, columns = out_weight.shape
    vmem = pl.BlockSpec(memory_space=pltpu.VMEM)
    hbm = pl.BlockSpec(memory_space=pl.ANY)
    dma = pltpu.SemaphoreType.DMA
    out = pl.pallas_call(
        functools.partial(kernel, sp, dp),
        out_shape=pltpu.VMEM((rows, columns * dp), jnp.bfloat16),
        in_specs=[hbm] * 8,
        out_specs=vmem,
        scratch_shapes=[
            pltpu.VMEM((2, length, width), jnp.bfloat16),
            pltpu.VMEM((2, length, width), jnp.bfloat16),
            pltpu.VMEM((length, vwidth), jnp.bfloat16),
            pltpu.VMEM((2, length, width), jnp.bfloat16),
            pltpu.VMEM((2, rows, sp // 2 * width), jnp.bfloat16),
            pltpu.VMEM((2, sp // 2 * rows, sp // 2 * width), jnp.bfloat16),
            pltpu.VMEM((sp // 2 * rows, sp // 2 * vwidth), jnp.bfloat16),
            pltpu.VMEM((2, sp // 2 * rows, width), jnp.bfloat16),
            pltpu.VMEM((sp, rows, vwidth), jnp.bfloat16),
            pltpu.VMEM((sp, rows, vwidth), jnp.bfloat16),
            pltpu.VMEM((dp, depth, columns), jnp.bfloat16),
            dma((10,)), dma((5 * sp * sp,)), dma((5 * sp * sp,)), dma((sp,)), dma((sp,)),
            dma((dp // 2, 2)), dma((dp // 2, 2)), dma((dp // 2,)), dma((dp // 2,)), dma,
            pltpu.SMEM(lambdas.shape, jnp.float32),
            pltpu.VMEM((1, HK), jnp.float32), pltpu.VMEM((1, HK), jnp.float32), pltpu.VMEM((1, HV), jnp.float32),
            dma((4,)),
            pltpu.VMEM((rows, columns * dp), jnp.float32),
        ],
        compiler_params=pltpu.CompilerParams(collective_id=0, has_side_effects=True),
    )(
        query_rows[0], key_rows[0], value_rows[0], lambdas,
        query_gain[None], key_gain[None], sub_gain[None], out_weight,
    )
    return out[None]


def solution(mesh):
    in_specs = (
        P("dp", "sp", None),
        P("dp", "sp", None),
        P("dp", "sp", None),
        P(),
        P(),
        P(),
        P(),
        P(None, "dp"),
    )
    out_specs = P("dp", "sp", None)
    sp, dp = mesh.shape["sp"], mesh.shape["dp"]

    def step(*operands):
        if fits(sp, dp, operands[0].shape, operands[7].shape):
            return fused(sp, dp, *operands)
        return body(*operands)

    return jax.shard_map(step, mesh=mesh, in_specs=in_specs, out_specs=out_specs, check_vma=False)
```

profile of v0, /device:TPU:24, one launch (start us, length us, event | category | flops | bytes accessed | tf_op | source)
XLA Modules:
  0.0 29.8 jit_solution(6421864550887947415)
XLA Ops:
  0.0 29.0 %shard_map.82 = bf16[128,2048]{1,0:T(8,128)(2,1)S(1)} custom-call(bf16[128,1024]{1,0:T(8,128)(2,1)} %bitcast.8, bf16[128,1024]{1,0:T(8,128)(2,1)} %bitcast.9, bf16[128,1024]{1,0:T(8,128)(2,1)} %bitcast.10, f32[8]{0:T(128)} %lam_in.1, f32[1,64]{1,0:T(1,128)} %bitcast.11, f32[1,64]{1,0:T(1,128)} %bitcast.12, f32[1,128]{1,0:T(1,128)} %bitcast.13, ...), custom_call_target="tpu_custom_call" | custom-call | tf_op jit(solution)/shard_map/pallas_call | solution.py:459
  29.0 0.8 %copy.10 = bf16[1,128,2048]{2,1,0:T(8,128)(2,1)} copy(bf16[1,128,2048]{2,1,0:T(8,128)(2,1)S(1)} %bitcast.7) | data formatting | bytes 1048576
where the time goes:
time: 29.9 us; the launch traced here: 29.8 us
  Pallas kernels  29 us (97%)
  local copies, waits for them, and re-layouts  0.8 us (3%)
    pallas_call x1, Pallas kernels, fused(): pl.pallas_call(functools.partial(kernel, sp, dp), out_shape=pltpu.VMEM((r...  29 us
    unnamed x1, local copies, waits for them, and re-layouts  0.8 us

commit v1 on v0

v1 whole, which is shorter than its diff:
```python
import functools

import jax
import jax.numpy as jnp
from jax import lax
from jax.experimental import pallas as pl
from jax.experimental.pallas import tpu as pltpu
from jax.sharding import PartitionSpec as P

D = 2048
HEADS = 8
HK = 64
HV = 128


epsilon = 1e-06
output_scale = 0.8


def normalize(field, scaling):
    return field * lax.rsqrt(jnp.mean(field * field, axis=-1, keepdims=True) + epsilon) * scaling


def attend(arrived, length):
    block_rows = max(min(512, length), length // 16)
    results = []
    for number in range(length // block_rows):
        first_row = number * block_rows
        last_row = first_row + block_rows
        query_block = arrived[first_row:last_row, :, :HK]
        key_block = arrived[:last_row, :, HK : 2 * HK]
        value_block = arrived[:last_row, :, 2 * HK :]
        scores = jnp.einsum(
            "qgd,kgd->gqk", query_block, key_block, preferred_element_type=jnp.float32
        ) * HK ** (-0.5)
        visible = jnp.arange(last_row)[None, :] <= (first_row + jnp.arange(block_rows))[:, None]
        scores = jnp.where(visible[None], scores, -jnp.inf)
        weights = jax.nn.softmax(scores, axis=-1).astype(jnp.bfloat16)
        results.append(
            jnp.einsum(
                "gqk,kgd->qgd", weights, value_block, preferred_element_type=jnp.float32
            ).astype(jnp.bfloat16)
        )
    return jnp.concatenate(results, axis=0)


def body(query_rows, key_rows, value_rows, lambdas, query_gain, key_gain, sub_gain, out_weight):
    sequences = query_rows.shape[0]
    tokens_here = query_rows.shape[1]
    groups = 2 * HEADS
    query_norm = normalize(
        query_rows.reshape(sequences, tokens_here, groups, HK).astype(jnp.float32), query_gain
    ).astype(jnp.bfloat16)
    key_norm = normalize(
        key_rows.reshape(sequences, tokens_here, groups, HK).astype(jnp.float32), key_gain
    ).astype(jnp.bfloat16)
    value_heads = value_rows.reshape(sequences, tokens_here, HEADS, HV)
    packet = jnp.concatenate(
        [query_norm, key_norm, jnp.concatenate([value_heads, value_heads], axis=2)], axis=3
    )
    arrived = lax.all_to_all(packet, "sp", split_axis=2, concat_axis=1, tiled=True)
    length = arrived.shape[1]
    map_outputs = attend(arrived[0], length)[None]
    returned = lax.all_to_all(map_outputs, "sp", split_axis=1, concat_axis=2, tiled=True)
    returned_float = returned.astype(jnp.float32)
    mixed_heads = returned_float[:, :, :HEADS] - lambdas[:, None] * returned_float[:, :, HEADS:]
    normed = (
        (normalize(mixed_heads, sub_gain) * output_scale)
        .astype(jnp.bfloat16)
        .reshape(sequences * tokens_here, HEADS * HV)
    )
    projected = jnp.dot(
        normed,
        lax.all_gather(out_weight, "dp", axis=1, tiled=True),
        preferred_element_type=jnp.float32,
    )
    return projected.astype(jnp.bfloat16).reshape(sequences, tokens_here, D)


MESH = pl.DeviceIdType.MESH
TILE = 2 * HK
EVERY = range(HEADS)
LOW, MIDDLE, TOP = (2, 0, 1), (4, 5, 3), (6, 7)
SPLIT = len(LOW) * HV
SEATS = 14


def fits(sp, dp, rows_shape, weight_shape):
    if sp != 4 or dp not in (2, 8) or HEADS != 8 or TILE != 128 or HV != TILE:
        return False
    return rows_shape[0] == 1 and rows_shape[1] % 128 == 0 and rows_shape[1] * sp <= 1024 and weight_shape[1] % 128 == 0


def routes():
    first = {
        0: [("kv", h, 0, 1, h) for h in TOP + MIDDLE + LOW],
        1: [("kv", h, 1, 2, h) for h in MIDDLE] + [("kv", h, 1, 3, h) for h in TOP],
        2: [("all", 2, 2, 1, HEADS), ("all", 6, 2, 3, HEADS), ("all", 7, 2, 3, HEADS + 1),
            ("all", 0, 2, 1, HEADS + 1), ("all", 1, 2, 1, HEADS + 2)],
        3: [("all", h, 3, 2, HEADS + n) for n, h in enumerate(LOW + MIDDLE)],
    }
    passed = {
        1: [("kv", h, 0, 3 if h in TOP else 2, h) for h in TOP + MIDDLE],
        2: [("all", h, 3, 1, HEADS + 3 + n) for n, h in enumerate(LOW)],
    }
    out = {
        1: [("out", h, 2 * n + r - 2, r, 7 if r == 2 else 11) for n, h in enumerate(LOW) for r in (3, 2)],
        2: [("out", h, n, 3, 10) for n, h in enumerate(MIDDLE)],
        3: [("out", h, n, 2, 6) for n, h in enumerate(TOP)],
    }
    return first, passed, out


def kernel(
    sp, dp, q_ref, k_ref, v_ref, lam_in, qg_in, kg_in, sg_in, w_ref, out_ref,
    raw, qkv, ob, nsend, wbuf, acc, lam_ref, qg_ref, kg_ref, sg_ref,
    raw_sem, v_sem, own_sem, small_sem, far_sem, send_sem, in_recv, w_recv, p_recv,
):
    me, d = lax.axis_index("sp"), lax.axis_index("dp")
    swap = 1 - 2 * lax.rem(d, 2)
    partner = d + swap
    chips = dp // 2
    square = chips == 4
    rows = q_ref.shape[0]
    depth, columns = w_ref.shape
    half = depth // 2
    first, passed, out = routes()

    def fellow(c):
        core, chip = lax.rem(d, 2), d // 2
        x, y = lax.rem(chip, 2), chip // 2
        x = 1 - x if c % 2 else x
        y = 1 - y if c // 2 else y
        return (y * 2 + x) * 2 + core

    def role(body):
        for z in range(sp):
            @pl.when(me == z)
            def _(z=z):
                body(z)

    barrier = pltpu.get_barrier_semaphore()

    def greet(z, device):
        pl.semaphore_signal(barrier, inc=1, device_id=(z, device), device_id_type=MESH)

    beside = (1, 2) if square else ()
    greet(me, partner)
    for c in beside:
        greet(me, fellow(c))

    def neighbours(z):
        return [n for n in (z - 1, z + 1) if 0 <= n < sp]

    def greet_line(z):
        for n in neighbours(z):
            greet(n, d)

    role(greet_line)

    small = [
        pltpu.make_async_copy(src, dst, small_sem.at[n])
        for n, (src, dst) in enumerate(((lam_in, lam_ref), (qg_in, qg_ref), (kg_in, kg_ref), (sg_in, sg_ref)))
    ]

    def rows_of(h):
        return pl.ds(h * half, half)

    def own_weights():
        return pltpu.make_async_copy(w_ref, wbuf.at[d], own_sem)

    for n, src in enumerate((k_ref, q_ref)):
        pltpu.make_async_copy(src, raw.at[n], raw_sem.at[n]).start()
    for copy in small:
        copy.start()
    own_weights().start()
    for h in EVERY:
        pltpu.make_async_copy(v_ref.at[:, pl.ds(h * HV, HV)], qkv.at[h, me, 1], v_sem).start()

    def remote(src, dst, recv, to):
        return pltpu.make_async_remote_copy(
            src_ref=src, dst_ref=dst, send_sem=send_sem, recv_sem=recv, device_id=to, device_id_type=MESH,
        )

    def spread(c, h):
        source, over = d, c
        if c == 3:
            source, over = fellow(1 + h), 2 - h
        piece = wbuf.at[source, rows_of(h)]
        return remote(piece, piece, w_recv.at[2 * c - 2 + h], (me, fellow(over)))

    def gained(c, h):
        piece = wbuf.at[fellow(c), rows_of(h)]
        remote(piece, piece, w_recv.at[2 * c - 2 + h], (me, partner)).wait_recv()

    def pair(c, h=None, at=None):
        at = fellow(c) if at is None else at
        piece = wbuf.at[at] if h is None else wbuf.at[at, rows_of(h)]
        return remote(piece, piece, p_recv.at[c + (h or 0)], (me, partner))

    def paired(c, h=None):
        pair(c, h, fellow(c) + swap).wait_recv()

    def put(key):
        kind, h, r, to, n = key
        if kind == "out":
            return remote(nsend.at[r], ob.at[:, pl.ds(h * HV, HV)], in_recv.at[n], (to, d))
        piece = qkv.at[h, r, pl.ds(0, 2)] if kind == "kv" else qkv.at[h, r]
        return remote(piece, piece, in_recv.at[n], (to, d))

    def got(piece, n):
        remote(piece, piece, in_recv.at[n], (me, partner)).wait_recv()

    def got_kv(h, count=1):
        got(qkv.at[h, 0, pl.ds(0, 2)] if count == 1 else qkv.at[h, pl.ds(0, 2), pl.ds(0, 2)], h)

    def got_all(h, r, n):
        got(qkv.at[h, r], HEADS + n)

    def weights_start():
        own_weights().wait()
        for order in range(2):
            for c in beside:
                spread(c, (c + 1 + order) % 2).start()
        pair(0).start()

    def weights_first():
        if square:
            for h in range(2):
                gained(1 + h, h)
                spread(3, h).start()

    def weights_next():
        if square:
            for h in range(2):
                gained(1 + h, 1 - h)
                pair(1 + h).start()

    def weights_last():
        if square:
            for h in range(2):
                gained(3, h)
                pair(3, h).start()

    pl.semaphore_wait(barrier, 1 + len(beside) + 2 - jnp.where((me == 0) | (me == sp - 1), 1, 0))

    @pl.when(me == 2)
    def _():
        pl.semaphore_signal(far_sem, inc=1, device_id=(1, d), device_id_type=MESH)

    weights_start()
    for copy in small:
        copy.wait()

    lane = lax.broadcasted_iota(jnp.int32, (2 * TILE, TILE), 1) // HK
    from_lane = lax.rem(lax.broadcasted_iota(jnp.int32, (2 * TILE, TILE), 0), TILE) // HK
    ones = (lane == from_lane).astype(jnp.bfloat16)
    early = lax.broadcasted_iota(jnp.int32, (rows, TILE), 1) < HK
    visible = lax.broadcasted_iota(jnp.int32, (rows, rows), 1) <= lax.broadcasted_iota(jnp.int32, (rows, rows), 0)
    visible = jnp.concatenate([visible] * 2, axis=0)
    gains = [jnp.concatenate([ref[...]] * 2, axis=1) for ref in (kg_ref, qg_ref)]
    sub_gain = sg_ref[...] * output_scale
    decay = HK ** (-0.5) * 1.4426950408889634

    def normed_rows(block, gain):
        field = block.astype(jnp.float32)
        square = field * field
        upper = square.astype(jnp.bfloat16)
        lower = (square - upper.astype(jnp.float32)).astype(jnp.bfloat16)
        total = jnp.dot(jnp.concatenate([upper, lower], axis=1), ones, preferred_element_type=jnp.float32)
        return field * lax.rsqrt(total * (1.0 / HK) + epsilon) * gain

    def own_rows(z, n, p):
        here = [
            normed_rows(raw[n, :, m * HEADS * HK + p * TILE : m * HEADS * HK + (p + 1) * TILE], gains[n])
            for m in range(2)
        ]
        there = [pltpu.roll(x, HK, axis=1) for x in here]
        qkv[2 * p, z, 2 * n] = jnp.where(early, here[0], there[1]).astype(jnp.bfloat16)
        qkv[2 * p + 1, z, 2 * n] = jnp.where(early, there[0], here[1]).astype(jnp.bfloat16)

    def unit(h, r):
        query = qkv[h, r, 2]
        zero = jnp.zeros_like(query)
        stacked = jnp.concatenate([jnp.where(early, query, zero), jnp.where(early, zero, query)], axis=0)
        keys = qkv[h, : r + 1, 0].reshape((r + 1) * rows, TILE)
        values = qkv[h, : r + 1, 1].reshape((r + 1) * rows, HV)
        scores = lax.dot_general(stacked, keys, (((1,), (1,)), ((), ())), preferred_element_type=jnp.float32)
        last = jnp.where(visible, scores[:, r * rows :], -jnp.inf)
        scores = last if r == 0 else jnp.concatenate([scores[:, : r * rows], last], axis=1)
        raised = jnp.exp2((scores - jnp.max(scores, axis=1, keepdims=True)) * decay)
        weights = (raised * (1.0 / jnp.sum(raised, axis=1, keepdims=True))).astype(jnp.bfloat16)
        maps = jnp.dot(weights, values, preferred_element_type=jnp.float32).astype(jnp.bfloat16).astype(jnp.float32)
        mixed = maps[:rows] - lam_ref[h] * maps[rows:]
        mean = jnp.mean(mixed * mixed, axis=1, keepdims=True)
        return (mixed * lax.rsqrt(mean + epsilon) * sub_gain).astype(jnp.bfloat16)

    def keep(h, r):
        ob[:, h * HV : (h + 1) * HV] = unit(h, r)

    def give(z, key):
        kind, h, slot, to, n = key
        nsend[slot] = unit(h, to)

    def start(keys):
        for key in keys:
            put(key).start()

    def rows_ready(n):
        pltpu.make_async_copy(raw.at[n], raw.at[n], raw_sem.at[n]).wait()

    def values_ready():
        pltpu.make_async_copy(qkv.at[:, me, 1], qkv.at[:, me, 1], v_sem).wait()

    def prepare(z, order):
        waiting = list(first[z])
        with_query = z > 1
        done = set()

        def flush():
            while waiting and waiting[0][1] in done:
                put(waiting.pop(0)).start()

        rows_ready(0)
        if with_query:
            rows_ready(1)
        for count, p in enumerate(order):
            own_rows(z, 0, p)
            if with_query:
                own_rows(z, 1, p)
            if count == 0:
                values_ready()
            if z == 1 and 2 * p in TOP:
                pl.semaphore_wait(far_sem, 1)
            done.update((2 * p, 2 * p + 1))
            flush()
        if not with_query:
            rows_ready(1)
            for p in order:
                own_rows(z, 1, p)

    def part(z):
        if z == 0:
            prepare(z, (3, 2, 1, 0))
            for h in EVERY:
                keep(h, 0)
            weights_first()
            weights_next()
        if z == 1:
            prepare(z, (2, 1, 3, 0))
            for n, key in enumerate(passed[1]):
                got_kv(key[1])
                put(key).start()
                keep(key[1], 1)
                if n == 2:
                    weights_first()
            for n, h in enumerate(LOW):
                got_kv(h)
                got_all(h, 2, n)
                got_all(h, 3, 3 + n)
                for key in out[1][2 * n : 2 * n + 2]:
                    give(z, key)
                keep(h, 1)
                start(out[1][2 * n : 2 * n + 2])
                if n == 1:
                    weights_next()
        if z == 2:
            prepare(z, (1, 3, 0, 2))
            for n, key in enumerate(passed[2]):
                got_all(key[1], 3, n)
                put(key).start()
            weights_first()
            for n, h in enumerate(MIDDLE):
                got_kv(h, 2)
                got_all(h, 3, 3 + n)
                give(z, out[2][n])
                keep(h, 2)
                put(out[2][n]).start()
                if n == 0:
                    weights_next()
        if z == 3:
            prepare(z, (1, 0, 2, 3))
            weights_first()
            for n, h in enumerate(TOP):
                got_kv(h, 2)
                got_all(h, 2, n)
                give(z, out[3][n])
                keep(h, 3)
                put(out[3][n]).start()
            weights_next()

    role(part)

    def project(shard, lower):
        where = slice(0, SPLIT) if lower else slice(SPLIT, depth)
        here = pl.ds(pl.multiple_of(shard * columns, 128), columns)
        total = jnp.dot(ob[:, where], wbuf[shard, where, :], preferred_element_type=jnp.float32)
        if lower:
            out_ref[:, here] = (acc[:, here] + total).astype(jnp.bfloat16)
        else:
            acc[:, here] = total

    def outputs(which):
        def body(z):
            if z == 2:
                if which:
                    got(ob.at[:, pl.ds(0, len(TOP) * HV)], 6)
                else:
                    got(ob.at[:, pl.ds(0, SPLIT)], 7)
            if z == 3:
                if which:
                    got(ob.at[:, pl.ds(0, len(MIDDLE) * HV)], 10)
                else:
                    got(ob.at[:, pl.ds(0, SPLIT)], 11)
        role(body)

    weights_last()
    outputs(True)
    paired(0)
    for c in beside:
        paired(c)
    for c in range(chips):
        project(fellow(c), False)
        if c < 3:
            project(fellow(c) + swap, False)
    if square:
        for h in range(2):
            paired(3, h)
        project(fellow(3) + swap, False)
    outputs(False)
    for c in range(chips):
        project(fellow(c), True)
        project(fellow(c) + swap, True)

    def drain(z):
        for keys in (first, passed, out):
            for key in keys.get(z, ()):
                put(key).wait_send()

    role(drain)
    pair(0).wait_send()
    if square:
        for c in range(1, chips):
            for h in range(2):
                spread(c, h).wait_send()
            pair(c).wait_send()


def fused(sp, dp, query_rows, key_rows, value_rows, lambdas, query_gain, key_gain, sub_gain, out_weight):
    rows = query_rows.shape[1]
    depth, columns = out_weight.shape
    vmem = pl.BlockSpec(memory_space=pltpu.VMEM)
    hbm = pl.BlockSpec(memory_space=pl.ANY)
    dma = pltpu.SemaphoreType.DMA
    out = pl.pallas_call(
        functools.partial(kernel, sp, dp),
        out_shape=pltpu.VMEM((rows, columns * dp), jnp.bfloat16),
        in_specs=[hbm] * 8,
        out_specs=vmem,
        scratch_shapes=[
            pltpu.VMEM((2, rows, 2 * HEADS * HK), jnp.bfloat16),
            pltpu.VMEM((HEADS, sp, 3, rows, TILE), jnp.bfloat16),
            pltpu.VMEM((rows, HEADS * HV), jnp.bfloat16),
            pltpu.VMEM((2 * len(LOW), rows, HV), jnp.bfloat16),
            pltpu.VMEM((dp, depth, columns), jnp.bfloat16),
            pltpu.VMEM((rows, columns * dp), jnp.float32),
            pltpu.SMEM(lambdas.shape, jnp.float32),
            pltpu.VMEM((1, HK), jnp.float32), pltpu.VMEM((1, HK), jnp.float32), pltpu.VMEM((1, HV), jnp.float32),
            dma((2,)), dma, dma, dma((4,)), pltpu.SemaphoreType.REGULAR, dma, dma((SEATS,)), dma((6,)), dma((5,)),
        ],
        compiler_params=pltpu.CompilerParams(collective_id=0, has_side_effects=True),
    )(
        query_rows[0], key_rows[0], value_rows[0], lambdas,
        query_gain[None], key_gain[None], sub_gain[None], out_weight,
    )
    return out[None]


def solution(mesh):
    in_specs = (
        P("dp", "sp", None),
        P("dp", "sp", None),
        P("dp", "sp", None),
        P(),
        P(),
        P(),
        P(),
        P(None, "dp"),
    )
    out_specs = P("dp", "sp", None)
    sp, dp = mesh.shape["sp"], mesh.shape["dp"]

    def step(*operands):
        if fits(sp, dp, operands[0].shape, operands[7].shape):
            return fused(sp, dp, *operands)
        return body(*operands)

    return jax.shard_map(step, mesh=mesh, in_specs=in_specs, out_specs=out_specs, check_vma=False)
```

time: 29.9 us -> 25.3 us (0.85)
  the two profiles are of different devices: /device:TPU:24 before, /device:TPU:1 now
where the time goes in v1:
time: 25.3 us; the launch traced here: 25.1 us
  Pallas kernels  24.3 us (96%)
  local copies, waits for them, and re-layouts  0.8 us (3%)
    pallas_call x1, Pallas kernels, fused(): pl.pallas_call(functools.partial(kernel, sp, dp), out_shape=pltpu.VMEM((r...  24.3 us
    unnamed x1, local copies, waits for them, and re-layouts  0.8 us

profile of v1, /device:TPU:1, one launch (start us, length us, event | category | flops | bytes accessed | tf_op | source)
XLA Modules:
  0.0 25.1 jit_solution(15417229202561195672)
XLA Ops:
  0.0 24.3 %shard_map.82 = bf16[128,2048]{1,0:T(8,128)(2,1)S(1)} custom-call(bf16[128,1024]{1,0:T(8,128)(2,1)} %bitcast.8, bf16[128,1024]{1,0:T(8,128)(2,1)} %bitcast.9, bf16[128,1024]{1,0:T(8,128)(2,1)} %bitcast.10, f32[8]{0:T(128)} %lam_in.1, f32[1,64]{1,0:T(1,128)} %bitcast.11, f32[1,64]{1,0:T(1,128)} %bitcast.12, f32[1,128]{1,0:T(1,128)} %bitcast.13, ...), custom_call_target="tpu_custom_call" | custom-call | tf_op jit(solution)/shard_map/pallas_call | solution.py:455
  24.3 0.8 %copy.10 = bf16[1,128,2048]{2,1,0:T(8,128)(2,1)} copy(bf16[1,128,2048]{2,1,0:T(8,128)(2,1)S(1)} %bitcast.7) | data formatting | bytes 1048576

commit v2 on v1

--- a/solution.py
+++ b/solution.py
@@ -80,8 +80,7 @@
 MESH = pl.DeviceIdType.MESH
 TILE = 2 * HK
 EVERY = range(HEADS)
-LOW, MIDDLE, TOP = (2, 0, 1), (4, 5, 3), (6, 7)
-SPLIT = len(LOW) * HV
+LOW, MIDDLE, TOP = (0, 1, 2), (4, 5, 3), (6, 7)
 SEATS = 14
 
 
@@ -93,10 +92,10 @@
 
 def routes():
     first = {
-        0: [("kv", h, 0, 1, h) for h in TOP + MIDDLE + LOW],
+        0: [("kv", h, 0, 1, h) for h in (6, 7, 0, 4, 5, 1, 3, 2)],
         1: [("kv", h, 1, 2, h) for h in MIDDLE] + [("kv", h, 1, 3, h) for h in TOP],
-        2: [("all", 2, 2, 1, HEADS), ("all", 6, 2, 3, HEADS), ("all", 7, 2, 3, HEADS + 1),
-            ("all", 0, 2, 1, HEADS + 1), ("all", 1, 2, 1, HEADS + 2)],
+        2: [("all", 0, 2, 1, HEADS), ("all", 1, 2, 1, HEADS + 1), ("all", 6, 2, 3, HEADS), ("all", 7, 2, 3, HEADS + 1),
+            ("all", 2, 2, 1, HEADS + 2)],
         3: [("all", h, 3, 2, HEADS + n) for n, h in enumerate(LOW + MIDDLE)],
     }
     passed = {
@@ -104,9 +103,10 @@
         2: [("all", h, 3, 1, HEADS + 3 + n) for n, h in enumerate(LOW)],
     }
     out = {
-        1: [("out", h, 2 * n + r - 2, r, 7 if r == 2 else 11) for n, h in enumerate(LOW) for r in (3, 2)],
-        2: [("out", h, n, 3, 10) for n, h in enumerate(MIDDLE)],
-        3: [("out", h, n, 2, 6) for n, h in enumerate(TOP)],
+        1: [("out", h, n, 2, 6 if n < 2 else 7) for n, h in enumerate(LOW)]
+        + [("out", h, 3 + n, 3, 10 if n < 2 else 11) for n, h in enumerate(LOW)],
+        2: [("out", h, n, 3, 12 if n < 2 else 13) for n, h in enumerate(MIDDLE)],
+        3: [("out", h, n, 2, 1) for n, h in enumerate(TOP)],
     }
     return first, passed, out
 
@@ -182,24 +182,31 @@
             src_ref=src, dst_ref=dst, send_sem=send_sem, recv_sem=recv, device_id=to, device_id_type=MESH,
         )
 
-    def spread(c, h):
+    def piece(device, h, j=None):
+        size = half if j is None else half // 2
+        return wbuf.at[device, pl.ds(h * half + (j or 0) * size, size)]
+
+    def seat(c, h, j=None):
+        return 2 * c - 2 + h if j is None else 4 + 2 * h + j
+
+    def spread(c, h, j=None):
         source, over = d, c
         if c == 3:
             source, over = fellow(1 + h), 2 - h
-        piece = wbuf.at[source, rows_of(h)]
-        return remote(piece, piece, w_recv.at[2 * c - 2 + h], (me, fellow(over)))
-
-    def gained(c, h):
-        piece = wbuf.at[fellow(c), rows_of(h)]
-        remote(piece, piece, w_recv.at[2 * c - 2 + h], (me, partner)).wait_recv()
-
-    def pair(c, h=None, at=None):
+        block = piece(source, h, j)
+        return remote(block, block, w_recv.at[seat(c, h, j)], (me, fellow(over)))
+
+    def gained(c, h, j=None):
+        block = piece(fellow(c), h, j)
+        remote(block, block, w_recv.at[seat(c, h, j)], (me, partner)).wait_recv()
+
+    def pair(c, h=None, j=None, at=None):
         at = fellow(c) if at is None else at
-        piece = wbuf.at[at] if h is None else wbuf.at[at, rows_of(h)]
-        return remote(piece, piece, p_recv.at[c + (h or 0)], (me, partner))
-
-    def paired(c, h=None):
-        pair(c, h, fellow(c) + swap).wait_recv()
+        block = wbuf.at[at] if h is None else piece(at, h, j)
+        return remote(block, block, p_recv.at[c + (2 * h + j if h is not None else 0)], (me, partner))
+
+    def paired(c, h=None, j=None):
+        pair(c, h, j, fellow(c) + swap).wait_recv()
 
     def put(key):
         kind, h, r, to, n = key
@@ -228,7 +235,8 @@
         if square:
             for h in range(2):
                 gained(1 + h, h)
-                spread(3, h).start()
+                for j in range(2):
+                    spread(3, h, j).start()
 
     def weights_next():
         if square:
@@ -238,17 +246,11 @@
 
     def weights_last():
         if square:
-            for h in range(2):
-                gained(3, h)
-                pair(3, h).start()
-
-    pl.semaphore_wait(barrier, 1 + len(beside) + 2 - jnp.where((me == 0) | (me == sp - 1), 1, 0))
-
-    @pl.when(me == 2)
-    def _():
-        pl.semaphore_signal(far_sem, inc=1, device_id=(1, d), device_id_type=MESH)
-
-    weights_start()
+            for j in range(2):
+                for h in range(2):
+                    gained(3, h, j)
+                    pair(3, h, j).start()
+
     for copy in small:
         copy.wait()
 
@@ -312,132 +314,183 @@
     def values_ready():
         pltpu.make_async_copy(qkv.at[:, me, 1], qkv.at[:, me, 1], v_sem).wait()
 
-    def prepare(z, order):
+    orders = {0: (3, 0, 2, 1), 1: (2, 1, 3, 0), 2: (0, 3, 1, 2), 3: (0, 1, 2, 3)}
+
+    def before(z):
+        rows_ready(0)
+        if z > 1:
+            rows_ready(1)
+        for n in range(2 if z > 1 else 1):
+            own_rows(z, n, orders[z][0])
+
+    role(before)
+    pl.semaphore_wait(barrier, 1 + len(beside) + 2 - jnp.where((me == 0) | (me == sp - 1), 1, 0))
+
+    @pl.when(me == 2)
+    def _():
+        pl.semaphore_signal(far_sem, inc=1, device_id=(1, d), device_id_type=MESH)
+
+    weights_start()
+    values_ready()
+
+    def prepare(z):
         waiting = list(first[z])
-        with_query = z > 1
         done = set()
-
-        def flush():
-            while waiting and waiting[0][1] in done:
-                put(waiting.pop(0)).start()
-
-        rows_ready(0)
-        if with_query:
-            rows_ready(1)
-        for count, p in enumerate(order):
-            own_rows(z, 0, p)
-            if with_query:
-                own_rows(z, 1, p)
-            if count == 0:
-                values_ready()
+        for count, p in enumerate(orders[z]):
+            if count:
+                for n in range(2 if z > 1 else 1):
+                    own_rows(z, n, p)
             if z == 1 and 2 * p in TOP:
                 pl.semaphore_wait(far_sem, 1)
             done.update((2 * p, 2 * p + 1))
-            flush()
-        if not with_query:
+            while waiting and waiting[0][1] in done:
+                put(waiting.pop(0)).start()
+        if z < 2:
             rows_ready(1)
-            for p in order:
+            for p in orders[z]:
                 own_rows(z, 1, p)
 
+    def project(shards, pieces, store):
+        for shard in shards:
+            here = pl.ds(pl.multiple_of(shard * columns, 128), columns)
+            total = None if "new" in store else acc[:, here]
+            for a, b in pieces:
+                where = slice(a * HV, b * HV)
+                part = jnp.dot(ob[:, where], wbuf[shard, where, :], preferred_element_type=jnp.float32)
+                total = part if total is None else total + part
+            if "end" in store:
+                out_ref[:, here] = total.astype(jnp.bfloat16)
+            else:
+                acc[:, here] = total
+
+    own = [fellow(c) for c in range(min(chips, 3))]
+    theirs = [fellow(c) + swap for c in range(min(chips, 3))]
+    last_own = [fellow(3)] if square else []
+    last_theirs = [fellow(3) + swap] if square else []
+
+    def weights_mid():
+        paired(0)
+        for c in beside:
+            paired(c)
+
+    def weights_end():
+        if square:
+            for j in range(2):
+                for h in range(2):
+                    paired(3, h, j)
+
+    whole = ((0, HEADS),)
+
+    def part_0():
+        for h in EVERY:
+            keep(h, 0)
+        paired(0)
+        project([own[0], theirs[0]], whole, "new end")
+        weights_first()
+        weights_next()
+        project(own[1:], whole, "new end")
+        for c in beside:
+            paired(c)
+        project(theirs[1:], whole, "new end")
+        weights_last()
+        project(last_own, whole, "new end")
+        weights_end()
+        project(last_theirs, whole, "new end")
+
+    def relay(n):
+        got_kv(passed[1][n][1])
+        put(passed[1][n]).start()
+        keep(passed[1][n][1], 1)
+
+    def lower_two(n):
+        got_kv(LOW[n])
+        got_all(LOW[n], 2, n)
+        keep(LOW[n], 1)
+        give(1, out[1][n])
+
+    def lower_three(n):
+        got_all(LOW[n], 3, 3 + n)
+        give(1, out[1][3 + n])
+        put(out[1][3 + n]).start()
+
+    def part_1():
+        relay(0)
+        relay(1)
+        lower_two(0)
+        relay(2)
+        weights_first()
+        relay(3)
+        lower_two(1)
+        relay(4)
+        start(out[1][:2])
+        lower_three(0)
+        lower_two(2)
+        lower_three(1)
+        put(out[1][2]).start()
+        weights_next()
+        lower_three(2)
+        weights_mid()
+        project(own + theirs, whole, "new end")
+        weights_last()
+        project(last_own, whole, "new end")
+        weights_end()
+        project(last_theirs, whole, "new end")
+
+    def part_2():
+        for n, key in enumerate(passed[2]):
+            got_all(key[1], 3, n)
+            put(key).start()
+        weights_first()
+        for n, h in enumerate(MIDDLE):
+            got_kv(h, 2)
+            got_all(h, 3, 3 + n)
+            give(2, out[2][n])
+            put(out[2][n]).start()
+            keep(h, 2)
+            if n == 0:
+                weights_next()
+        weights_mid()
+        got(ob.at[:, pl.ds(0, 2 * HV)], 1)
+        project(own + theirs, ((4, 8),), "new")
+        weights_last()
+        got(ob.at[:, pl.ds(0, 2 * HV)], 6)
+        project(own + theirs, ((0, 2),), "")
+        project(last_own, ((0, 2), (4, 8)), "new")
+        weights_end()
+        project(last_theirs, ((0, 2), (4, 8)), "new")
+        got(ob.at[:, pl.ds(0, HV)], 7)
+        project(own + theirs + last_own + last_theirs, ((2, 4),), "end")
+
+    def part_3():
+        weights_first()
+        for n, h in enumerate(TOP):
+            got_kv(h, 2)
+            got_all(h, 2, n)
+            give(3, out[3][n])
+            put(out[3][n]).start()
+            keep(h, 3)
+        weights_next()
+        weights_mid()
+        project(own + theirs, ((6, 8),), "new")
+        weights_last()
+        got(ob.at[:, pl.ds(0, 2 * HV)], 12)
+        got(ob.at[:, pl.ds(0, 2 * HV)], 10)
+        project(own + theirs, ((0, 2), (4, 6)), "")
+        project(last_own, ((0, 2), (4, 8)), "new")
+        weights_end()
+        project(last_theirs, ((0, 2), (4, 8)), "new")
+        got(ob.at[:, pl.ds(0, HV)], 13)
+        got(ob.at[:, pl.ds(0, HV)], 11)
+        project(own + theirs + last_own + last_theirs, ((2, 4),), "end")
+
     def part(z):
-        if z == 0:
-            prepare(z, (3, 2, 1, 0))
-            for h in EVERY:
-                keep(h, 0)
-            weights_first()
-            weights_next()
-        if z == 1:
-            prepare(z, (2, 1, 3, 0))
-            for n, key in enumerate(passed[1]):
-                got_kv(key[1])
-                put(key).start()
-                keep(key[1], 1)
-                if n == 2:
-                    weights_first()
-            for n, h in enumerate(LOW):
-                got_kv(h)
-                got_all(h, 2, n)
-                got_all(h, 3, 3 + n)
-                for key in out[1][2 * n : 2 * n + 2]:
-                    give(z, key)
-                keep(h, 1)
-                start(out[1][2 * n : 2 * n + 2])
-                if n == 1:
-                    weights_next()
-        if z == 2:
-            prepare(z, (1, 3, 0, 2))
-            for n, key in enumerate(passed[2]):
-                got_all(key[1], 3, n)
-                put(key).start()
-            weights_first()
-            for n, h in enumerate(MIDDLE):
-                got_kv(h, 2)
-                got_all(h, 3, 3 + n)
-                give(z, out[2][n])
-                keep(h, 2)
-                put(out[2][n]).start()
-                if n == 0:
-                    weights_next()
-        if z == 3:
-            prepare(z, (1, 0, 2, 3))
-            weights_first()
-            for n, h in enumerate(TOP):
-                got_kv(h, 2)
-                got_all(h, 2, n)
-                give(z, out[3][n])
-                keep(h, 3)
-                put(out[3][n]).start()
-            weights_next()
-
-    role(part)
-
-    def project(shard, lower):
-        where = slice(0, SPLIT) if lower else slice(SPLIT, depth)
-        here = pl.ds(pl.multiple_of(shard * columns, 128), columns)
-        total = jnp.dot(ob[:, where], wbuf[shard, where, :], preferred_element_type=jnp.float32)
-        if lower:
-            out_ref[:, here] = (acc[:, here] + total).astype(jnp.bfloat16)
-        else:
-            acc[:, here] = total
-
-    def outputs(which):
-        def body(z):
-            if z == 2:
-                if which:
-                    got(ob.at[:, pl.ds(0, len(TOP) * HV)], 6)
-                else:
-                    got(ob.at[:, pl.ds(0, SPLIT)], 7)
-            if z == 3:
-                if which:
-                    got(ob.at[:, pl.ds(0, len(MIDDLE) * HV)], 10)
-                else:
-                    got(ob.at[:, pl.ds(0, SPLIT)], 11)
-        role(body)
-
-    weights_last()
-    outputs(True)
-    paired(0)
-    for c in beside:
-        paired(c)
-    for c in range(chips):
-        project(fellow(c), False)
-        if c < 3:
-            project(fellow(c) + swap, False)
-    if square:
-        for h in range(2):
-            paired(3, h)
-        project(fellow(3) + swap, False)
-    outputs(False)
-    for c in range(chips):
-        project(fellow(c), True)
-        project(fellow(c) + swap, True)
-
-    def drain(z):
+        prepare(z)
+        (part_0, part_1, part_2, part_3)[z]()
         for keys in (first, passed, out):
             for key in keys.get(z, ()):
                 put(key).wait_send()
 
-    role(drain)
+    role(part)
     pair(0).wait_send()
     if square:
         for c in range(1, chips):
@@ -466,7 +519,7 @@
             pltpu.VMEM((rows, columns * dp), jnp.float32),
             pltpu.SMEM(lambdas.shape, jnp.float32),
             pltpu.VMEM((1, HK), jnp.float32), pltpu.VMEM((1, HK), jnp.float32), pltpu.VMEM((1, HV), jnp.float32),
-            dma((2,)), dma, dma, dma((4,)), pltpu.SemaphoreType.REGULAR, dma, dma((SEATS,)), dma((6,)), dma((5,)),
+            dma((2,)), dma, dma, dma((4,)), pltpu.SemaphoreType.REGULAR, dma, dma((SEATS,)), dma((8,)), dma((7,)),
         ],
         compiler_params=pltpu.CompilerParams(collective_id=0, has_side_effects=True),
     )(

time: 25.3 us -> 24.7 us (0.976)
  Pallas kernels: 24.3 us -> 23.8 us
    pallas_call x1, Pallas kernels: 24.3 us -> 23.8 us  [fused(): pl.pallas_call(functools.partial(kernel, sp, dp), out_shape=pltpu.VMEM((r...]
where the time goes in v2:
time: 24.7 us; the launch traced here: 24.6 us
  Pallas kernels  23.8 us (96%)
  local copies, waits for them, and re-layouts  0.8 us (3%)
    pallas_call x1, Pallas kernels, fused(): pl.pallas_call(functools.partial(kernel, sp, dp), out_shape=pltpu.VMEM((r...  23.8 us
    unnamed x1, local copies, waits for them, and re-layouts  0.8 us

profile of v2, /device:TPU:1, one launch (start us, length us, event | category | flops | bytes accessed | tf_op | source)
XLA Modules:
  0.0 24.6 jit_solution(9683193190654369429)
XLA Ops:
  0.0 23.8 %shard_map.82 = bf16[128,2048]{1,0:T(8,128)(2,1)S(1)} custom-call(bf16[128,1024]{1,0:T(8,128)(2,1)} %bitcast.8, bf16[128,1024]{1,0:T(8,128)(2,1)} %bitcast.9, bf16[128,1024]{1,0:T(8,128)(2,1)} %bitcast.10, f32[8]{0:T(128)} %lam_in.1, f32[1,64]{1,0:T(1,128)} %bitcast.11, f32[1,64]{1,0:T(1,128)} %bitcast.12, f32[1,128]{1,0:T(1,128)} %bitcast.13, ...), custom_call_target="tpu_custom_call" | custom-call | tf_op jit(solution)/shard_map/pallas_call | solution.py:508
  23.8 0.8 %copy.10 = bf16[1,128,2048]{2,1,0:T(8,128)(2,1)} copy(bf16[1,128,2048]{2,1,0:T(8,128)(2,1)S(1)} %bitcast.7) | data formatting | bytes 1048576
